TPU v7x, 32 devices: a whole 2x2x4 slice. The times are simulated.
32 devices in a mesh: sp: 8 (over z, x), tp: 4 (over y, core).
Axes of the slice: x: 2, y: 2, z: 4, core: 2. Of those that a mesh axis runs over, the one named last changes fastest.
Arguments:
- cotangent: bfloat16 [1024, 2048], P('sp'), may hold values from -6 to 6
- mixer_out: bfloat16 [1024, 2048], P('sp'), may hold values from -6 to 6
- expert_ids: int32 [1024, 2], P('sp'), may hold values from 0 to 7, all different within a row; in each aligned block of 128 rows (0 to 127, 128 to 255, ...) at most 64 rows name the same one
- route_weight: float32 [1024, 2], P('sp'), may hold values from 0.3 to 1.5
- saved_normalized: bfloat16 [1024, 2048], P('sp', 'tp'), may hold values from -6 to 6
- inverse_deviation: float32 [1024], P('sp'), may hold values from 0.3 to 3
- channel_norm_gain: float32 [2048], P('tp'), may hold values from 0.1 to 1.9
- taps: float32 [31, 2048], P(None, 'tp'), may hold values from -1 to 1
- proj_weight: bfloat16 [2048, 2048], P('tp'), may hold values from -0.125 to 0.125
- gate_weight: bfloat16 [8, 2048, 2048], P('sp', None, 'tp'), may hold values from -0.125 to 0.125
- up_weight: bfloat16 [8, 2048, 2048], P('sp', None, 'tp'), may hold values from -0.125 to 0.125
- down_weight: bfloat16 [8, 2048, 2048], P('sp', 'tp'), may hold values from -0.125 to 0.125
Outputs:
- grad_mixer_in: bfloat16 [1024, 2048], P('sp', 'tp')
- grad_proj: float32 [2048, 2048], P('sp', 'tp')
- grad_gate: bfloat16 [8, 2048, 2048], P('sp', None, 'tp')
- grad_up: bfloat16 [8, 2048, 2048], P('sp', None, 'tp')
- grad_down: bfloat16 [8, 2048, 2048], P('sp', 'tp')
Inputs may be any that keep to these rules, and one draw needn't show every extreme that they name: `expert_ids`: each row names 2 different experts. Within the rows of one index of sp no expert is named more than 64 times, a bound that some block reaches.
All inputs are finite; a program needn't handle non-finite values.
Results may differ from a plain program's by a relative error of at most 0.02.
Values may be sent and summed in bfloat16 or wider, within the bound.
A program may use at most 64 MiB of HBM per device.

v0:
```python
import jax
import jax.numpy as jnp
from jax import lax
from jax.sharding import PartitionSpec as P


def from_behind(value, axis, steps):
    count = lax.axis_size(axis)
    leading, last = (max(0, -steps), min(count, count - steps))
    return lax.ppermute(value, axis, [(source, source + steps) for source in range(leading, last)])


def route_table(expert_ids, route_weight, slot_start, slot_span, capacity, experts):
    onehot = (expert_ids[:, :, None] == jnp.arange(experts, dtype=jnp.int32)[None, None, :]).astype(
        jnp.int32
    )
    flat_hot = onehot.reshape(-1, experts)
    ranks = jnp.cumsum(flat_hot, axis=0) - flat_hot
    rank_pair = jnp.sum(ranks * flat_hot, axis=1).reshape(expert_ids.shape)
    slot_index = expert_ids * capacity + rank_pair
    targets = (
        jnp.arange(experts, dtype=jnp.int32)[:, None] * capacity
        + slot_start
        + jnp.arange(slot_span, dtype=jnp.int32)[None, :]
    ).reshape(-1)
    matched = slot_index[None, :, :] == targets[:, None, None]
    dispatch = jnp.any(matched, axis=2).astype(jnp.bfloat16)
    slot_weight = jnp.sum(jnp.where(matched, route_weight[None, :, :], 0.0), axis=(1, 2))
    return (dispatch, slot_weight)


def shards(
    cotangent,
    mixer_out,
    expert_ids,
    route_weight,
    saved_normalized,
    inverse_deviation,
    channel_norm_gain,
    taps,
    proj_weight,
    gate_weight,
    up_weight,
    down_weight,
):
    experts = lax.axis_size("sp")
    groups = lax.axis_size("tp")
    tok_rows, model_width = cotangent.shape
    capacity = groups * max(1, 4 * tok_rows // (experts * groups))
    slot_span = capacity // groups
    slot_start = lax.axis_index("tp") * slot_span
    dispatch, slot_weight = route_table(
        expert_ids, route_weight, slot_start, slot_span, capacity, experts
    )
    sent_rows = jnp.dot(dispatch, mixer_out, preferred_element_type=jnp.float32).astype(
        jnp.bfloat16
    )
    sent_grad = (
        slot_weight[:, None] * jnp.dot(dispatch, cotangent, preferred_element_type=jnp.float32)
    ).astype(jnp.bfloat16)
    sent_rows = sent_rows.reshape(experts, slot_span, model_width)
    sent_grad = sent_grad.reshape(experts, slot_span, model_width)
    shared_rows = (
        lax.all_to_all(sent_rows, "sp", split_axis=0, concat_axis=0, tiled=True),
        lax.all_to_all(sent_grad, "sp", split_axis=0, concat_axis=0, tiled=True),
    )
    routed_rows, routed_grad = (
        lax.all_gather(shared_rows[0], "tp", axis=1, tiled=True),
        lax.all_gather(shared_rows[1], "tp", axis=1, tiled=True),
    )
    full_table, unused_weight = route_table(
        expert_ids, route_weight, 0, capacity, capacity, experts
    )
    routed_rows = routed_rows.reshape(-1, model_width)
    routed_grad = routed_grad.reshape(-1, model_width)
    w_first = gate_weight[0]
    w_third = up_weight[0]
    w_second = down_weight[0]
    contract_last = (((1,), (1,)), ((), ()))
    contract_first = (((0,), (0,)), ((), ()))
    hidden_gate = jnp.dot(routed_rows, w_first, preferred_element_type=jnp.float32)
    hidden_up = jnp.dot(routed_rows, w_third, preferred_element_type=jnp.float32)
    sigma = jax.nn.sigmoid(hidden_gate)
    swish = hidden_gate * sigma
    activ = (swish * hidden_up).astype(jnp.bfloat16)
    grad_second = lax.dot_general(
        activ, routed_grad, contract_first, preferred_element_type=jnp.float32
    ).astype(jnp.bfloat16)
    grad_activ = lax.dot_general(
        routed_grad, w_second, contract_last, preferred_element_type=jnp.float32
    )
    grad_gpre = (grad_activ * hidden_up * sigma * (1.0 + hidden_gate * (1.0 - sigma))).astype(
        jnp.bfloat16
    )
    grad_upre = (grad_activ * swish).astype(jnp.bfloat16)
    grad_first = lax.dot_general(
        routed_rows, grad_gpre, contract_first, preferred_element_type=jnp.float32
    ).astype(jnp.bfloat16)
    grad_third = lax.dot_general(
        routed_rows, grad_upre, contract_first, preferred_element_type=jnp.float32
    ).astype(jnp.bfloat16)
    partial_value = lax.dot_general(
        grad_gpre, w_first, contract_last, preferred_element_type=jnp.float32
    ) + lax.dot_general(grad_upre, w_third, contract_last, preferred_element_type=jnp.float32)
    summed = lax.psum(partial_value.astype(jnp.bfloat16), "tp")
    home_rows = lax.all_to_all(
        summed.reshape(experts, capacity, model_width),
        "sp",
        split_axis=0,
        concat_axis=0,
        tiled=True,
    )
    returned = lax.dot_general(
        full_table,
        home_rows.reshape(-1, model_width),
        contract_first,
        preferred_element_type=jnp.float32,
    )
    mixer_grad = (cotangent.astype(jnp.float32) + returned).astype(jnp.bfloat16)
    normalized_input = saved_normalized.astype(jnp.float32)
    normalized_values = normalized_input * channel_norm_gain[None, :]
    gate_sig = jax.nn.sigmoid(normalized_values)
    act_conv = (normalized_values * gate_sig).astype(jnp.bfloat16)
    grad_proj = lax.psum_scatter(
        lax.dot_general(
            mixer_grad, act_conv, contract_first, preferred_element_type=jnp.float32
        ).astype(jnp.bfloat16),
        "sp",
        scatter_dimension=0,
        tiled=True,
    ).astype(jnp.float32)
    grad_act = lax.dot_general(
        mixer_grad, proj_weight, contract_last, preferred_element_type=jnp.float32
    )
    norm_output_gradient = (
        grad_act
        * gate_sig
        * (1.0 + normalized_values * (1.0 - gate_sig))
        * channel_norm_gain[None, :]
    )
    reduced_totals = lax.psum(
        (
            jnp.sum(norm_output_gradient, axis=1),
            jnp.sum(norm_output_gradient * normalized_input, axis=1),
        ),
        "tp",
    )
    channel_count = saved_normalized.shape[1] * groups
    conv_output_gradient = inverse_deviation[:, None] * (
        norm_output_gradient
        - reduced_totals[0][:, None] / channel_count
        - normalized_input * (reduced_totals[1][:, None] / channel_count)
    )
    reach = taps.shape[0] - 1
    beyond = from_behind(conv_output_gradient[:reach], "sp", -1)
    extended = jnp.concatenate([conv_output_gradient, beyond], axis=0)
    result = jnp.zeros_like(conv_output_gradient)
    for tap_index in range(taps.shape[0]):
        result = result + taps[tap_index][None, :] * extended[tap_index : tap_index + tok_rows]
    return (
        result.astype(jnp.bfloat16),
        grad_proj,
        grad_first[None],
        grad_third[None],
        grad_second[None],
    )


def solution(mesh):
    return jax.shard_map(
        shards,
        mesh=mesh,
        in_specs=(
            P("sp", None),
            P("sp", None),
            P("sp", None),
            P("sp", None),
            P("sp", "tp"),
            P("sp"),
            P("tp"),
            P(None, "tp"),
            P("tp", None),
            P("sp", None, "tp"),
            P("sp", None, "tp"),
            P("sp", "tp", None),
        ),
        out_specs=(
            P("sp", "tp"),
            P("sp", "tp"),
            P("sp", None, "tp"),
            P("sp", None, "tp"),
            P("sp", "tp", None),
        ),
        check_vma=False,
    )
```

profile of v0, /device:TPU:0, one launch (start us, length us, event | category | flops | bytes accessed | tf_op | source)
XLA Modules:
  0.0 273.1 jit_solution(8081440627756328696)
XLA Ops:
  10.6 1.3 convolution_convert_fusion.4
  11.9 21.7 %all_to_all.15 = bf16[8,16,2048]{2,1,0:T(8,128)(2,1)} all-to-all(bf16[8,16,2048]{2,1,0:T(8,128)(2,1)S(1)} %bitcast.87), channel_id=1, replica_groups=mesh['sp'=8,'tp'=4] {'sp'}, dimensions={0} | all-to-all | bytes 1048576 | tf_op jit(solution)/shard_map/all_to_all | solution.py:64
  34.2 17.6 %all_to_all.16 = bf16[8,16,2048]{2,1,0:T(8,128)(2,1)} all-to-all(bf16[8,16,2048]{2,1,0:T(8,128)(2,1)S(1)} %bitcast.86), channel_id=1, replica_groups=mesh['sp'=8,'tp'=4] {'sp'}, dimensions={0} | all-to-all | bytes 1048576 | tf_op jit(solution)/shard_map/all_to_all | solution.py:65
  51.9 3.5 %all-gather.5.cloned.1.call-done = bf16[8,64,2048]{2,1,0:T(8,128)(2,1)} async-done(((bf16[8,16,2048]{2,1,0:T(8,128)(2,1)}), bf16[8,64,2048]{2,1,0:T(8,128)(2,1)}) %all-gather.5.cloned.1.call-update) | async-done | bytes 2097168 | tf_op jit(solution)/shard_map/all_gather | solution.py:68
  55.4 4.0 %fusion.7 = f32[512,512]{1,0:T(8,128)} fusion(bf16[512,2048]{1,0:T(8,128)(2,1)} %bitcast.119, bf16[1,2048,512]{2,1,0:T(8,128)(2,1)S(1)} %copy-done), kind=kOutput, calls=%fused_computation.44 | convolution fusion | flops 1073741824 | bytes 5242880 | tf_op jit(solution)/shard_map/dot_general | solution.py:81
  59.4 2.3 fusion.10
  61.7 17.9 %all-gather.3.cloned.1.call-done = bf16[8,64,2048]{2,1,0:T(8,128)(2,1)} async-done(((bf16[8,16,2048]{2,1,0:T(8,128)(2,1)}), bf16[8,64,2048]{2,1,0:T(8,128)(2,1)}) %all-gather.3.cloned.1.call-update) | async-done | bytes 2097168 | tf_op jit(solution)/shard_map/all_gather | solution.py:69
  79.6 4.4 %multiply_convert_fusion.1 = (bf16[512,512]{1,0:T(8,128)(2,1)S(1)}, bf16[512,512]{1,0:T(8,128)(2,1)S(1)}) fusion(f32[512,512]{1,0:T(8,128)} %fusion.7, f32[512,512]{1,0:T(8,128)} %fusion.10, bf16[512,2048]{1,0:T(8,128)(2,1)} %bitcast.123, bf16[1,512,2048]{2,1,0:T(8,128)(2,1)} %param.23), kind=kOutput, calls=%fused_computation.55 | convolution fusion | flops 1077149696 | bytes 7340032 | tf_op jit(solution)/shard_map/dot_general | solution.py:89
  84.0 1.3 fusion.5
  85.9 2.6 add_convert_fusion
  88.6 51.5 %all-reduce.3.cloned.1.call-done = bf16[8,64,2048]{2,1,0:T(8,128)(2,1)} async-done(((bf16[8,64,2048]{2,1,0:T(8,128)(2,1)}), bf16[8,64,2048]{2,1,0:T(8,128)(2,1)}) %all-reduce.3.cloned.1.call-update) | async-done | bytes 2097168 | tf_op jit(solution)/shard_map/psum | solution.py:105
  140.1 5.5 %all-to-all-start.2 = ((bf16[8,64,2048]{2,1,0:T(8,128)(2,1)}), bf16[8,64,2048]{2,1,0:T(8,128)(2,1)}, u32[]{:S(2)}, u32[]{:S(2)}) async-start(bf16[8,64,2048]{2,1,0:T(8,128)(2,1)} %all-reduce.3.cloned.1.call-done), calls=%async_computation.2 | async-start | bytes 4194304 | tf_op jit(solution)/shard_map/all_to_all | solution.py:106
  146.0 47.7 %all-to-all-done.2 = bf16[8,64,2048]{2,1,0:T(8,128)(2,1)} async-done(((bf16[8,64,2048]{2,1,0:T(8,128)(2,1)}), bf16[8,64,2048]{2,1,0:T(8,128)(2,1)}, u32[]{:S(2)}, u32[]{:S(2)}) %all-to-all-start.2) | async-done | bytes 2097184 | tf_op jit(solution)/shard_map/all_to_all | solution.py:106
  193.7 2.1 fusion.4
  195.8 2.1 convolution_convert_fusion
  199.3 4.4 %fusion.1 = bf16[1,2048,512]{2,1,0:T(8,128)(2,1)} fusion(bf16[512,2048]{1,0:T(8,128)(2,1)} %bitcast.120, bf16[512,512]{1,0:T(8,128)(2,1)S(1)} %copy-done.7), kind=kOutput, calls=%fused_computation.35 | convolution fusion | flops 1074790400 | bytes 4718592 | tf_op jit(solution)/shard_map/dot_general | solution.py:99
  203.7 2.7 fusion.2
  206.4 1.5 fusion.128
  207.9 6.2 %all-reduce = (f32[128]{0:T(128)S(1)}, f32[128]{0:T(128)S(1)}) all-reduce(f32[128]{0:T(128)} %get-tuple-element.6, f32[128]{0:T(128)} %get-tuple-element.5), channel_id=1, replica_groups=mesh['sp'=8,'tp'=4] {'tp'}, use_global_device_ids=true, to_apply=%region_10.11 | all-reduce | flops 256 | bytes 2048 | tf_op jit(solution)/shard_map/psum | solution.py:141
  215.2 1.3 collective-permute-start
  216.5 4.3 %fusion = bf16[1,2048,512]{2,1,0:T(8,128)(2,1)} fusion(bf16[512,2048]{1,0:T(8,128)(2,1)} %bitcast.121, bf16[512,512]{1,0:T(8,128)(2,1)S(1)} %copy-done.5), kind=kOutput, calls=%fused_computation.34 | convolution fusion | flops 1074790400 | bytes 4718592 | tf_op jit(solution)/shard_map/dot_general | solution.py:96
  221.9 2.0 fusion.32
  223.9 40.9 %reduce-scatter.2.cloned.1.call-done = bf16[256,512]{1,0:T(8,128)(2,1)} async-done(((bf16[2048,512]{1,0:T(8,128)(2,1)}), bf16[256,512]{1,0:T(8,128)(2,1)}) %reduce-scatter.2.cloned.1.call-update) | async-done | bytes 262160 | tf_op jit(solution)/shard_map/reduce_scatter | solution.py:124
  264.8 1.8 convert_element_type.72
  (126 shorter events, 8.1 us)
Async XLA Ops:
  7.2 48.3 %copy-start = (bf16[1,2048,512]{2,1,0:T(8,128)(2,1)S(1)}, bf16[1,2048,512]{2,1,0:T(8,128)(2,1)}, u32[]{:S(2)}) copy-start(bf16[1,2048,512]{2,1,0:T(8,128)(2,1)} %param.21) | copy-start | bytes 6291460
  7.2 26.5 %copy-start.39 = (f32[128,2]{0,1:T(2,128)S(1)}, f32[128,2]{0,1:T(2,128)}, u32[]{:S(2)}) copy-start(f32[128,2]{0,1:T(2,128)} %param.15) | copy-start | bytes 3076
  7.2 26.7 %copy-start.3 = (bf16[128,2048]{1,0:T(8,128)(2,1)S(1)}, bf16[128,2048]{1,0:T(8,128)(2,1)}, u32[]{:S(2)}) copy-start(bf16[128,2048]{1,0:T(8,128)(2,1)} %param.12) | copy-start | bytes 1572868
  7.2 48.2 %all-gather.5.cloned.1.call-start = ((), (), s32[]{:S(2)}) async-start(), calls=%async_computation.5 | async-start | bytes 2621440 | tf_op jit(solution)/shard_map/all_gather | solution.py:68
  33.7 45.9 %all-gather.3.cloned.1.call-start = ((), (), s32[]{:S(2)}) async-start(), calls=%async_computation.4 | async-start | bytes 2621440 | tf_op jit(solution)/shard_map/all_gather | solution.py:69
  51.9 88.2 %all-reduce.3.cloned.1.call-start = ((), (), s32[]{:S(2)}) async-start(), calls=%async_computation.6 | async-start | bytes 4194304 | tf_op jit(solution)/shard_map/psum | solution.py:105
  140.1 53.6 %all-to-all-start.2 = ((bf16[8,64,2048]{2,1,0:T(8,128)(2,1)}), bf16[8,64,2048]{2,1,0:T(8,128)(2,1)}, u32[]{:S(2)}, u32[]{:S(2)}) async-start(bf16[8,64,2048]{2,1,0:T(8,128)(2,1)} %all-reduce.3.cloned.1.call-done), calls=%async_computation.2 | async-start | bytes 4194304 | tf_op jit(solution)/shard_map/all_to_all | solution.py:106
  145.6 50.2 %copy-start.8 = (bf16[128,512]{1,0:T(8,128)(2,1)S(1)}, bf16[128,512]{1,0:T(8,128)(2,1)}, u32[]{:S(2)}) copy-start(bf16[128,512]{1,0:T(8,128)(2,1)} %param.16) | copy-start | bytes 393220
  145.6 50.2 %copy-start.37 = (f32[512]{0:T(512)S(1)}, f32[512]{0:T(512)}, u32[]{:S(2)}) copy-start(f32[512]{0:T(512)} %param.18) | copy-start | bytes 6148
  145.6 119.1 %reduce-scatter.2.cloned.1.call-start = ((), (), s32[]{:S(2)}) async-start(), calls=%async_computation.7 | async-start | bytes 2359296 | tf_op jit(solution)/shard_map/reduce_scatter | solution.py:124
  206.4 10.0 %copy-start.5 = (bf16[512,512]{1,0:T(8,128)(2,1)S(1)}, bf16[512,512]{1,0:T(8,128)(2,1)}, u32[]{:S(2)}) copy-start(bf16[512,512]{1,0:T(8,128)(2,1)} %copy-done.4) | copy-start | bytes 1572868
  214.9 6.8 %copy-start.10 = (f32[1,512]{1,0:T(1,128)S(1)}, f32[1,512]{1,0:T(1,128)}, u32[]{:S(2)}) copy-start(f32[1,512]{1,0:T(1,128)} %get-tuple-element.34) | copy-start | bytes 6148
  214.9 6.8 %copy-start.11 = (f32[1,512]{1,0:T(1,128)S(1)}, f32[1,512]{1,0:T(1,128)}, u32[]{:S(2)}) copy-start(f32[1,512]{1,0:T(1,128)} %get-tuple-element.35) | copy-start | bytes 6148
  214.9 6.8 %copy-start.12 = (f32[1,512]{1,0:T(1,128)S(1)}, f32[1,512]{1,0:T(1,128)}, u32[]{:S(2)}) copy-start(f32[1,512]{1,0:T(1,128)} %get-tuple-element.36) | copy-start | bytes 6148
  214.9 6.8 %copy-start.13 = (f32[1,512]{1,0:T(1,128)S(1)}, f32[1,512]{1,0:T(1,128)}, u32[]{:S(2)}) copy-start(f32[1,512]{1,0:T(1,128)} %get-tuple-element.37) | copy-start | bytes 6148
  214.9 6.8 %copy-start.14 = (f32[1,512]{1,0:T(1,128)S(1)}, f32[1,512]{1,0:T(1,128)}, u32[]{:S(2)}) copy-start(f32[1,512]{1,0:T(1,128)} %get-tuple-element.38) | copy-start | bytes 6148
  214.9 6.8 %copy-start.15 = (f32[1,512]{1,0:T(1,128)S(1)}, f32[1,512]{1,0:T(1,128)}, u32[]{:S(2)}) copy-start(f32[1,512]{1,0:T(1,128)} %get-tuple-element.39) | copy-start | bytes 6148
  214.9 6.8 %copy-start.16 = (f32[1,512]{1,0:T(1,128)S(1)}, f32[1,512]{1,0:T(1,128)}, u32[]{:S(2)}) copy-start(f32[1,512]{1,0:T(1,128)} %get-tuple-element.40) | copy-start | bytes 6148
  215.0 6.8 %copy-start.17 = (f32[1,512]{1,0:T(1,128)S(1)}, f32[1,512]{1,0:T(1,128)}, u32[]{:S(2)}) copy-start(f32[1,512]{1,0:T(1,128)} %get-tuple-element.41) | copy-start | bytes 6148
  215.0 6.8 %copy-start.18 = (f32[1,512]{1,0:T(1,128)S(1)}, f32[1,512]{1,0:T(1,128)}, u32[]{:S(2)}) copy-start(f32[1,512]{1,0:T(1,128)} %get-tuple-element.11) | copy-start | bytes 6148
  215.0 6.8 %copy-start.19 = (f32[1,512]{1,0:T(1,128)S(1)}, f32[1,512]{1,0:T(1,128)}, u32[]{:S(2)}) copy-start(f32[1,512]{1,0:T(1,128)} %get-tuple-element.12) | copy-start | bytes 6148
  215.0 6.8 %copy-start.20 = (f32[1,512]{1,0:T(1,128)S(1)}, f32[1,512]{1,0:T(1,128)}, u32[]{:S(2)}) copy-start(f32[1,512]{1,0:T(1,128)} %get-tuple-element.13) | copy-start | bytes 6148
  215.0 6.8 %copy-start.21 = (f32[1,512]{1,0:T(1,128)S(1)}, f32[1,512]{1,0:T(1,128)}, u32[]{:S(2)}) copy-start(f32[1,512]{1,0:T(1,128)} %get-tuple-element.14) | copy-start | bytes 6148
  215.2 6.5 %collective-permute-start = (f32[30,512]{1,0:T(8,128)S(1)}, f32[30,512]{1,0:T(8,128)S(1)}, u32[]{:S(2)}, u32[]{:S(2)}) collective-permute-start(f32[30,512]{1,0:T(8,128)S(1)} %slice.257), channel_id=1, source_target_pairs={{4,0},{8,4},{12,8},{16,12},{20,16},{24,20},{28,24},{5,1},{9,5},{13... | collective-permute-start | bytes 184328 | tf_op jit(solution)/shard_map/ppermute | solution.py:10
  (27 other events, 138.3 us)
Sparse Core Ops, SparseCore 0:
  33.8 21.5 all-gather.4
  57.0 22.5 all-gather.2
  88.7 51.3 all-reduce.2
  198.1 66.5 reduce-scatter.1
where the time goes:
time: 274 us; the launch traced here: 273 us
  waiting for transfers between devices  163 us (59%)
  blocking collectives  45.5 us (17%)
  matrix products  33.1 us (12%)
  between operations  14.5 us (5%)
  starting transfers between devices  6.96 us (3%)
  other arithmetic  6.52 us (2%)
  local copies, waits for them, and re-layouts  3.94 us (1%)
    psum x1, waiting for transfers between devices, shards(): summed = lax.psum(partial_value.astype(jnp.bfloat16), 'tp')  51.5 us
    all_to_all x1, waiting for transfers between devices, shards(): lax.all_to_all(summed.reshape(experts, capacity, model_width), 'sp', spli...  47.7 us
    reduce_scatter x1, waiting for transfers between devices, shards(): lax.psum_scatter(lax.dot_general(mixer_grad, act_conv, contract_first, pr...  40.9 us
    all_to_all x1, blocking collectives, shards(): lax.all_to_all(sent_rows, 'sp', split_axis=0, concat_axis=0, tiled=True)  21.7 us
    all_gather x1, waiting for transfers between devices, shards(): lax.all_gather(shared_rows[1], 'tp', axis=1, tiled=True)  17.9 us
    all_to_all x1, blocking collectives, shards(): lax.all_to_all(sent_grad, 'sp', split_axis=0, concat_axis=0, tiled=True)  17.6 us
    psum x1, blocking collectives, shards(): lax.psum((jnp.sum(norm_output_gradient, axis=1), jnp.sum(norm_output_grad...  6.16 us
    all_to_all x1, starting transfers between devices, shards(): lax.all_to_all(summed.reshape(experts, capacity, model_width), 'sp', spli...  5.51 us
  transfers between devices with their start and end apart: 6, of which 6 were waited for; matrix products, arithmetic and copies ran while one was open for 9% of the time, Pallas kernels for 0%

commit v1 on v0

--- a/solution.py
+++ b/solution.py
@@ -2,6 +2,10 @@
 import jax.numpy as jnp
 from jax import lax
 from jax.sharding import PartitionSpec as P
+
+
+def press_classes(vals):
+    return jnp.concatenate(jax.lax.all_gather(vals, axis_name="tp"), 1)
 
 
 def from_behind(value, axis, steps):
@@ -66,7 +70,7 @@
     )
     routed_rows, routed_grad = (
         lax.all_gather(shared_rows[0], "tp", axis=1, tiled=True),
-        lax.all_gather(shared_rows[1], "tp", axis=1, tiled=True),
+        press_classes(shared_rows[1]),
     )
     full_table, unused_weight = route_table(
         expert_ids, route_weight, 0, capacity, capacity, experts

time: 274 us -> 277 us (1.011)
  matrix products: 33.1 us -> 28.5 us
  local copies, waits for them, and re-layouts: 3.94 us -> 8.19 us
  waiting for transfers between devices: 163 us -> 166 us
    all_gather x1, waiting for transfers between devices: 3.5 us -> 21 us  [shards(): lax.all_gather(shared_rows[0], 'tp', axis=1, tiled=True)]
    all_gather x1, waiting for transfers between devices: 17.9 us -> 3.68 us  [press_classes(): return jnp.concatenate(jax.lax.all_gather(vals, axis_name='tp'), 1)]
    all_to_all x1, blocking collectives: 17.6 us -> 21.7 us  [shards(): lax.all_to_all(sent_grad, 'sp', split_axis=0, concat_axis=0, tiled=True)]
    all_to_all x1, blocking collectives: 21.7 us -> 17.6 us  [shards(): lax.all_to_all(sent_rows, 'sp', split_axis=0, concat_axis=0, tiled=True)]
    reshape x0 -> x1, local copies, waits for them, and re-layouts: none -> 3.16 us  [press_classes(): return jnp.concatenate(jax.lax.all_gather(vals, axis_name='tp'), 1)]
  transfers between devices with their start and end apart: 6 -> 6, of which waited for: 6 -> 6; matrix products, arithmetic and copies ran while one was open for 9% -> 7% of each run, Pallas kernels for 0% -> 0%
where the time goes in v1:
time: 277 us
  waiting for transfers between devices  166 us (60%)
  blocking collectives  45.7 us (16%)
  matrix products  28.5 us (10%)
  between operations  14.5 us (5%)
  local copies, waits for them, and re-layouts  8.19 us (3%)
  other arithmetic  7.2 us (3%)
  starting transfers between devices  6.96 us (3%)
    psum x1, waiting for transfers between devices, shards(): summed = lax.psum(partial_value.astype(jnp.bfloat16), 'tp')  51.5 us
    all_to_all x1, waiting for transfers between devices, shards(): lax.all_to_all(summed.reshape(experts, capacity, model_width), 'sp', spli...  47.7 us
    reduce_scatter x1, waiting for transfers between devices, shards(): lax.psum_scatter(lax.dot_general(mixer_grad, act_conv, contract_first, pr...  41.1 us
    all_to_all x1, blocking collectives, shards(): lax.all_to_all(sent_grad, 'sp', split_axis=0, concat_axis=0, tiled=True)  21.7 us
    all_gather x1, waiting for transfers between devices, shards(): lax.all_gather(shared_rows[0], 'tp', axis=1, tiled=True)  21 us
    all_to_all x1, blocking collectives, shards(): lax.all_to_all(sent_rows, 'sp', split_axis=0, concat_axis=0, tiled=True)  17.6 us
    psum x1, blocking collectives, shards(): lax.psum((jnp.sum(norm_output_gradient, axis=1), jnp.sum(norm_output_grad...  6.34 us
  transfers between devices with their start and end apart: 6, of which 6 were waited for; matrix products, arithmetic and copies ran while one was open for 7% of the time, Pallas kernels for 0%

profile of v1, /device:TPU:0, one launch (start us, length us, event | category | flops | bytes accessed | tf_op | source)
XLA Modules:
  0.0 276.9 jit_solution(1488121317966146279)
XLA Ops:
  11.5 1.3 fusion.3
  12.8 21.7 %all_to_all.15 = bf16[8,16,2048]{2,1,0:T(8,128)(2,1)} all-to-all(bf16[8,16,2048]{2,1,0:T(8,128)(2,1)S(1)} %bitcast.92), channel_id=1, replica_groups=mesh['sp'=8,'tp'=4] {'sp'}, dimensions={0} | all-to-all | bytes 1048576 | tf_op jit(solution)/shard_map/all_to_all | solution.py:69
  34.9 17.6 %all_to_all.16 = bf16[8,16,2048]{2,1,0:T(8,128)(2,1)} all-to-all(bf16[8,16,2048]{2,1,0:T(8,128)(2,1)S(1)} %bitcast.93), channel_id=1, replica_groups=mesh['sp'=8,'tp'=4] {'sp'}, dimensions={0} | all-to-all | bytes 1048576 | tf_op jit(solution)/shard_map/all_to_all | solution.py:68
  52.6 3.7 %all-gather.6.cloned.1.call-done = bf16[32,16,2048]{2,1,0:T(8,128)(2,1)} async-done(((bf16[8,16,2048]{2,1,0:T(8,128)(2,1)}), bf16[32,16,2048]{2,1,0:T(8,128)(2,1)}) %all-gather.6.cloned.1.call-update) | async-done | bytes 2097168 | tf_op jit(solution)/shard_map/all_gather | solution.py:8
  56.3 3.2 %copy.47 = bf16[8,4,16,2048]{3,2,1,0:T(8,128)(2,1)} copy(bf16[8,4,16,2048]{3,2,0,1:T(8,128)(2,1)} %bitcast.91) | data formatting | bytes 4194304 | tf_op jit(solution)/shard_map/reshape | solution.py:8
  59.5 21.0 %all-gather.4.cloned.1.call-done = bf16[8,64,2048]{2,1,0:T(8,128)(2,1)} async-done(((bf16[8,16,2048]{2,1,0:T(8,128)(2,1)}), bf16[8,64,2048]{2,1,0:T(8,128)(2,1)}) %all-gather.4.cloned.1.call-update) | async-done | bytes 2097168 | tf_op jit(solution)/shard_map/all_gather | solution.py:72
  80.5 3.0 %fusion.7 = f32[512,512]{1,0:T(8,128)S(1)} fusion(bf16[512,2048]{1,0:T(8,128)(2,1)} %bitcast.125, bf16[1,2048,512]{2,1,0:T(8,128)(2,1)S(1)} %copy-done), kind=kOutput, calls=%fused_computation.44 | convolution fusion | flops 1073741824 | bytes 5242880 | tf_op jit(solution)/shard_map/dot_general | solution.py:85
  86.5 1.7 multiply_convert_fusion.1
  88.2 1.3 fusion.5
  89.5 2.6 add_convert_fusion
  92.1 51.5 %all-reduce.3.cloned.1.call-done = bf16[8,64,2048]{2,1,0:T(8,128)(2,1)} async-done(((bf16[8,64,2048]{2,1,0:T(8,128)(2,1)}), bf16[8,64,2048]{2,1,0:T(8,128)(2,1)}) %all-reduce.3.cloned.1.call-update) | async-done | bytes 2097168 | tf_op jit(solution)/shard_map/psum | solution.py:109
  143.7 5.5 %all-to-all-start.2 = ((bf16[8,64,2048]{2,1,0:T(8,128)(2,1)}), bf16[8,64,2048]{2,1,0:T(8,128)(2,1)}, u32[]{:S(2)}, u32[]{:S(2)}) async-start(bf16[8,64,2048]{2,1,0:T(8,128)(2,1)} %all-reduce.3.cloned.1.call-done), calls=%async_computation.2 | async-start | bytes 4194304 | tf_op jit(solution)/shard_map/all_to_all | solution.py:110
  149.6 47.7 %all-to-all-done.2 = bf16[8,64,2048]{2,1,0:T(8,128)(2,1)} async-done(((bf16[8,64,2048]{2,1,0:T(8,128)(2,1)}), bf16[8,64,2048]{2,1,0:T(8,128)(2,1)}, u32[]{:S(2)}, u32[]{:S(2)}) %all-to-all-start.2) | async-done | bytes 2097184 | tf_op jit(solution)/shard_map/all_to_all | solution.py:110
  197.3 2.1 fusion.4
  199.4 2.1 convolution_convert_fusion
  202.9 4.4 %fusion.1 = bf16[1,2048,512]{2,1,0:T(8,128)(2,1)} fusion(bf16[512,2048]{1,0:T(8,128)(2,1)} %bitcast.126, bf16[512,512]{1,0:T(8,128)(2,1)S(1)} %copy-done.8), kind=kOutput, calls=%fused_computation.35 | convolution fusion | flops 1074790400 | bytes 4718592 | tf_op jit(solution)/shard_map/dot_general | solution.py:103
  207.3 2.7 fusion.2
  210.0 1.6 fusion.128
  211.6 6.3 %all-reduce = (f32[128]{0:T(128)S(1)}, f32[128]{0:T(128)S(1)}) all-reduce(f32[128]{0:T(128)} %get-tuple-element.6, f32[128]{0:T(128)} %get-tuple-element.5), channel_id=1, replica_groups=mesh['sp'=8,'tp'=4] {'tp'}, use_global_device_ids=true, to_apply=%region_10.11 | all-reduce | flops 256 | bytes 2048 | tf_op jit(solution)/shard_map/psum | solution.py:145
  219.0 1.3 collective-permute-start
  220.3 4.3 %fusion = bf16[1,2048,512]{2,1,0:T(8,128)(2,1)} fusion(bf16[512,2048]{1,0:T(8,128)(2,1)} %bitcast.127, bf16[512,512]{1,0:T(8,128)(2,1)S(1)} %copy-done.6), kind=kOutput, calls=%fused_computation.34 | convolution fusion | flops 1074790400 | bytes 4718592 | tf_op jit(solution)/shard_map/dot_general | solution.py:100
  225.5 2.0 fusion.32
  227.5 41.1 %reduce-scatter.2.cloned.1.call-done = bf16[256,512]{1,0:T(8,128)(2,1)} async-done(((bf16[2048,512]{1,0:T(8,128)(2,1)}), bf16[256,512]{1,0:T(8,128)(2,1)}) %reduce-scatter.2.cloned.1.call-update) | async-done | bytes 262160 | tf_op jit(solution)/shard_map/reduce_scatter | solution.py:128
  268.6 1.8 convert_element_type.72
  (133 shorter events, 10.9 us)
Async XLA Ops:
  7.2 73.3 %copy-start = (bf16[1,2048,512]{2,1,0:T(8,128)(2,1)S(1)}, bf16[1,2048,512]{2,1,0:T(8,128)(2,1)}, u32[]{:S(2)}) copy-start(bf16[1,2048,512]{2,1,0:T(8,128)(2,1)} %param.21) | copy-start | bytes 6291460
  7.2 27.4 %copy-start.9 = (bf16[128,2048]{1,0:T(8,128)(2,1)S(1)}, bf16[128,2048]{1,0:T(8,128)(2,1)}, u32[]{:S(2)}) copy-start(bf16[128,2048]{1,0:T(8,128)(2,1)} %param.13) | copy-start | bytes 1572868
  7.2 49.1 %all-gather.6.cloned.1.call-start = ((), (), s32[]{:S(2)}) async-start(), calls=%async_computation.7 | async-start | bytes 2621440 | tf_op jit(solution)/shard_map/all_gather | solution.py:8
  34.6 45.9 %all-gather.4.cloned.1.call-start = ((), (), s32[]{:S(2)}) async-start(), calls=%async_computation.4 | async-start | bytes 2621440 | tf_op jit(solution)/shard_map/all_gather | solution.py:72
  52.6 91.1 %all-reduce.3.cloned.1.call-start = ((), (), s32[]{:S(2)}) async-start(), calls=%async_computation.5 | async-start | bytes 4194304 | tf_op jit(solution)/shard_map/psum | solution.py:109
  92.1 105.2 %copy-start.2 = (bf16[128,2048]{1,0:T(8,128)(2,1)S(1)}, bf16[128,2048]{1,0:T(8,128)(2,1)}, u32[]{:S(2)}) copy-start(bf16[128,2048]{1,0:T(8,128)(2,1)} %param.12) | copy-start | bytes 1572868
  143.7 53.6 %all-to-all-start.2 = ((bf16[8,64,2048]{2,1,0:T(8,128)(2,1)}), bf16[8,64,2048]{2,1,0:T(8,128)(2,1)}, u32[]{:S(2)}, u32[]{:S(2)}) async-start(bf16[8,64,2048]{2,1,0:T(8,128)(2,1)} %all-reduce.3.cloned.1.call-done), calls=%async_computation.2 | async-start | bytes 4194304 | tf_op jit(solution)/shard_map/all_to_all | solution.py:110
  149.2 50.2 %copy-start.10 = (bf16[128,512]{1,0:T(8,128)(2,1)S(1)}, bf16[128,512]{1,0:T(8,128)(2,1)}, u32[]{:S(2)}) copy-start(bf16[128,512]{1,0:T(8,128)(2,1)} %param.16) | copy-start | bytes 393220
  149.2 50.2 %copy-start.39 = (f32[512]{0:T(512)S(1)}, f32[512]{0:T(512)}, u32[]{:S(2)}) copy-start(f32[512]{0:T(512)} %param.18) | copy-start | bytes 6148
  149.2 119.4 %reduce-scatter.2.cloned.1.call-start = ((), (), s32[]{:S(2)}) async-start(), calls=%async_computation.6 | async-start | bytes 2359296 | tf_op jit(solution)/shard_map/reduce_scatter | solution.py:128
  210.0 10.3 %copy-start.6 = (bf16[512,512]{1,0:T(8,128)(2,1)S(1)}, bf16[512,512]{1,0:T(8,128)(2,1)}, u32[]{:S(2)}) copy-start(bf16[512,512]{1,0:T(8,128)(2,1)} %copy-done.5) | copy-start | bytes 1572868
  218.7 6.5 %copy-start.12 = (f32[1,512]{1,0:T(1,128)S(1)}, f32[1,512]{1,0:T(1,128)}, u32[]{:S(2)}) copy-start(f32[1,512]{1,0:T(1,128)} %get-tuple-element.34) | copy-start | bytes 6148
  218.8 6.5 %copy-start.13 = (f32[1,512]{1,0:T(1,128)S(1)}, f32[1,512]{1,0:T(1,128)}, u32[]{:S(2)}) copy-start(f32[1,512]{1,0:T(1,128)} %get-tuple-element.35) | copy-start | bytes 6148
  218.8 6.5 %copy-start.14 = (f32[1,512]{1,0:T(1,128)S(1)}, f32[1,512]{1,0:T(1,128)}, u32[]{:S(2)}) copy-start(f32[1,512]{1,0:T(1,128)} %get-tuple-element.36) | copy-start | bytes 6148
  218.8 6.5 %copy-start.15 = (f32[1,512]{1,0:T(1,128)S(1)}, f32[1,512]{1,0:T(1,128)}, u32[]{:S(2)}) copy-start(f32[1,512]{1,0:T(1,128)} %get-tuple-element.37) | copy-start | bytes 6148
  218.8 6.5 %copy-start.16 = (f32[1,512]{1,0:T(1,128)S(1)}, f32[1,512]{1,0:T(1,128)}, u32[]{:S(2)}) copy-start(f32[1,512]{1,0:T(1,128)} %get-tuple-element.38) | copy-start | bytes 6148
  218.8 6.5 %copy-start.17 = (f32[1,512]{1,0:T(1,128)S(1)}, f32[1,512]{1,0:T(1,128)}, u32[]{:S(2)}) copy-start(f32[1,512]{1,0:T(1,128)} %get-tuple-element.39) | copy-start | bytes 6148
  218.8 6.5 %copy-start.18 = (f32[1,512]{1,0:T(1,128)S(1)}, f32[1,512]{1,0:T(1,128)}, u32[]{:S(2)}) copy-start(f32[1,512]{1,0:T(1,128)} %get-tuple-element.40) | copy-start | bytes 6148
  218.8 6.5 %copy-start.19 = (f32[1,512]{1,0:T(1,128)S(1)}, f32[1,512]{1,0:T(1,128)}, u32[]{:S(2)}) copy-start(f32[1,512]{1,0:T(1,128)} %get-tuple-element.41) | copy-start | bytes 6148
  218.8 6.5 %copy-start.20 = (f32[1,512]{1,0:T(1,128)S(1)}, f32[1,512]{1,0:T(1,128)}, u32[]{:S(2)}) copy-start(f32[1,512]{1,0:T(1,128)} %get-tuple-element.11) | copy-start | bytes 6148
  218.8 6.5 %copy-start.21 = (f32[1,512]{1,0:T(1,128)S(1)}, f32[1,512]{1,0:T(1,128)}, u32[]{:S(2)}) copy-start(f32[1,512]{1,0:T(1,128)} %get-tuple-element.12) | copy-start | bytes 6148
  218.8 6.5 %copy-start.22 = (f32[1,512]{1,0:T(1,128)S(1)}, f32[1,512]{1,0:T(1,128)}, u32[]{:S(2)}) copy-start(f32[1,512]{1,0:T(1,128)} %get-tuple-element.13) | copy-start | bytes 6148
  218.9 6.5 %copy-start.23 = (f32[1,512]{1,0:T(1,128)S(1)}, f32[1,512]{1,0:T(1,128)}, u32[]{:S(2)}) copy-start(f32[1,512]{1,0:T(1,128)} %get-tuple-element.14) | copy-start | bytes 6148
  219.0 6.2 %collective-permute-start = (f32[30,512]{1,0:T(8,128)S(1)}, f32[30,512]{1,0:T(8,128)S(1)}, u32[]{:S(2)}, u32[]{:S(2)}) collective-permute-start(f32[30,512]{1,0:T(8,128)S(1)} %slice.257), channel_id=1, source_target_pairs={{4,0},{8,4},{12,8},{16,12},{20,16},{24,20},{28,24},{5,1},{9,5},{13... | collective-permute-start | bytes 184328 | tf_op jit(solution)/shard_map/ppermute | solution.py:14
  (30 other events, 140.1 us)
Sparse Core Ops, SparseCore 0:
  34.7 21.5 all-gather.5
  57.9 22.5 all-gather.3
  92.3 51.3 all-reduce.2
  201.7 66.8 reduce-scatter.1
